TPU v7x, 32 devices: a whole 2x2x4 slice. The times are simulated.
32 devices in a mesh: grp: 2 (over y), sp: 4 (over z), tp: 4 (over x, core).
Axes of the slice: x: 2, y: 2, z: 4, core: 2. Of those that a mesh axis runs over, the one named last changes fastest.
Arguments:
- tokens: bfloat16 [3072, 2048], P(('grp', 'sp'), 'tp'), parts along dimension 0, may hold values from -15 to 15
- gate_weight: bfloat16 [2, 2048, 2048], P(None, 'sp', 'tp'), may hold values from -0.125 to 0.125
- inner_weight: bfloat16 [2, 2048, 2048], P(None, 'sp', 'tp'), may hold values from -0.125 to 0.125
- value_weight: bfloat16 [2, 2048, 2048], P(None, 'sp', 'tp'), may hold values from -0.125 to 0.125
- out_weight: bfloat16 [2, 2048, 2048], P(None, 'tp', 'sp'), may hold values from -0.125 to 0.125
- taps: bfloat16 [2, 3, 2048], P(None, None, 'tp'), may hold values from -3 to 3
- norm_gain: float32 [2, 2048], P(None, 'tp'), may hold values from 0.1 to 1.9
- norm_bias: float32 [2, 2048], P(None, 'tp'), may hold values from -1.5 to 1.5
Outputs:
- mixed: bfloat16 [3072, 2048], P(('grp', 'sp'), 'tp'), parts along dimension 0
There are 2 independent parts, one for each index of `grp`. A program takes and returns all parts, laid end to end along the dimension named above; an argument that names none is the same for every part. Nothing has to cross between parts.
All inputs are finite; a program needn't handle non-finite values.
Results may differ from a plain program's by a relative error of at most 0.03.
Values may be sent and summed in bfloat16 or wider, within the bound.
A program may use at most 64 MiB of HBM per device.

v0:
```python
import jax
import jax.numpy as jnp
from jax import lax
from jax.sharding import PartitionSpec as P

LAYERS = 2


def extended(value, sides, width):
    for axis, dim in sides:
        peers, length = (lax.axis_size(axis), value.shape[dim])
        up = [(i, (i + 1) % peers) for i in range(peers - 1)]
        down = [(j, i) for i, j in up]
        last = lax.slice_in_dim(value, length - width, length, axis=dim)
        initial = lax.slice_in_dim(value, 0, width, axis=dim)
        before = lax.ppermute(last, axis, up)
        after = lax.ppermute(initial, axis, down)
        value = jnp.concatenate([before, value, after], axis=dim)
    return value


def shards(tokens, gate_weight, inner_weight, value_weight, out_weight, taps, norm_gain, norm_bias):
    x = tokens
    width = x.shape[1] * lax.axis_size("tp")
    full_gate, full_inner, full_value, full_out = (
        lax.all_gather(gate_weight, "sp", axis=1, tiled=True),
        lax.all_gather(inner_weight, "sp", axis=1, tiled=True),
        lax.all_gather(value_weight, "sp", axis=1, tiled=True),
        lax.all_gather(out_weight, "sp", axis=2, tiled=True),
    )
    for layer in range(LAYERS):
        whole = lax.all_gather(x, "tp", axis=1, tiled=True)
        outer = jnp.dot(whole, full_gate[layer], preferred_element_type=jnp.float32)
        inner = jnp.dot(whole, full_inner[layer], preferred_element_type=jnp.float32)
        values = jnp.dot(whole, full_value[layer], preferred_element_type=jnp.float32)
        outer = outer.astype(jnp.bfloat16)
        inner = inner.astype(jnp.bfloat16)
        values = values.astype(jnp.bfloat16)
        product = (inner.astype(jnp.float32) * values.astype(jnp.float32)).astype(jnp.bfloat16)
        padded = extended(product, (("sp", 0),), 1).astype(jnp.float32)
        kernel = taps[layer].astype(jnp.float32)
        conv = kernel[0] * padded[:-2] + kernel[1] * padded[1:-1] + kernel[2] * padded[2:]
        gated = (outer.astype(jnp.float32) * conv).astype(jnp.bfloat16)
        terms = jnp.dot(gated, full_out[layer], preferred_element_type=jnp.float32)
        branch = lax.psum_scatter(
            terms.astype(jnp.bfloat16), "tp", scatter_dimension=1, tiled=True
        ).astype(jnp.float32)
        total = 2.0**0.5 * x.astype(jnp.float32) + branch
        row_sum, row_square = lax.psum(
            (jnp.sum(total, axis=1), jnp.sum(total * total, axis=1)), "tp"
        )
        mean = (row_sum / width)[:, None]
        spread = (row_square / width)[:, None] - mean * mean
        x = (
            (total - mean) * lax.rsqrt(spread + 1e-05) * norm_gain[layer] + norm_bias[layer]
        ).astype(jnp.bfloat16)
    return x


def solution(mesh):
    in_specs = (
        P(("grp", "sp"), "tp"),
        P(None, "sp", "tp"),
        P(None, "sp", "tp"),
        P(None, "sp", "tp"),
        P(None, "tp", "sp"),
        P(None, None, "tp"),
        P(None, "tp"),
        P(None, "tp"),
    )
    out_specs = P(("grp", "sp"), "tp")
    return jax.shard_map(shards, mesh=mesh, in_specs=in_specs, out_specs=out_specs, check_vma=False)
```

profile of v0, /device:TPU:0, one launch (start us, length us, event | category | flops | bytes accessed | tf_op | source)
XLA Modules:
  0.0 479.8 jit_solution(8200364497382368189)
XLA Ops:
  6.5 0.0 all-gather.7.cloned.1.call-start
  6.5 0.7 all-gather.7.cloned.1.call-update
  7.3 0.0 copy-start.2
  7.3 0.0 all-gather.13.cloned.1.call-start
  7.3 0.7 all-gather.13.cloned.1.call-update
  8.0 0.0 all-gather.11.cloned.1.call-start
  8.1 0.7 all-gather.11.cloned.1.call-update
  8.8 0.0 all-gather.15.cloned.1.call-start
  8.8 0.5 all-gather.15.cloned.1.call-update
  9.3 0.0 all-gather.9.cloned.1.call-start
  9.4 0.5 all-gather.9.cloned.1.call-update
  9.9 0.0 reduce-scatter.3.cloned.1.call-start
  10.0 0.0 copy-done.2
  10.0 21.3 %all-gather.7.cloned.1.call-done = bf16[384,2048]{1,0:T(8,128)(2,1)} async-done(((bf16[384,512]{1,0:T(8,128)(2,1)}), bf16[384,2048]{1,0:T(8,128)(2,1)}) %all-gather.7.cloned.1.call-update) | async-done | bytes 1572880 | tf_op jit(solution)/shard_map/all_gather | solution.py:32
  31.3 0.0 copy-start.6
  31.3 82.3 %all-gather.13.cloned.1.call-done = bf16[2,2048,512]{2,1,0:T(8,128)(2,1)} async-done(((bf16[2,512,512]{2,1,0:T(8,128)(2,1)}), bf16[2,2048,512]{2,1,0:T(8,128)(2,1)}) %all-gather.13.cloned.1.call-update) | async-done | bytes 4194320 | tf_op jit(solution)/shard_map/all_gather | solution.py:28
  113.6 3.0 fusion.15
  116.7 77.8 %all-gather.11.cloned.1.call-done = bf16[2,2048,512]{2,1,0:T(8,128)(2,1)} async-done(((bf16[2,512,512]{2,1,0:T(8,128)(2,1)}), bf16[2,2048,512]{2,1,0:T(8,128)(2,1)}) %all-gather.11.cloned.1.call-update) | async-done | bytes 4194320 | tf_op jit(solution)/shard_map/all_gather | solution.py:27
  194.5 0.0 copy-done.6
  194.5 2.6 fusion.13
  197.0 1.3 collective-permute-start
  198.3 1.3 collective-permute-start.1
  199.7 0.0 collective-permute-done
  199.7 4.2 collective-permute-done.1
  203.9 0.1 maximum_convert_fusion
  204.0 71.1 %all-gather.15.cloned.1.call-done = bf16[2,512,2048]{2,1,0:T(8,128)(2,1)} async-done(((bf16[2,512,512]{2,1,0:T(8,128)(2,1)}), bf16[2,512,2048]{2,1,0:T(8,128)(2,1)}) %all-gather.15.cloned.1.call-update) | async-done | bytes 4194320 | tf_op jit(solution)/shard_map/all_gather | solution.py:29
  275.1 80.7 %all-gather.9.cloned.1.call-done = bf16[2,2048,512]{2,1,0:T(8,128)(2,1)} async-done(((bf16[2,512,512]{2,1,0:T(8,128)(2,1)}), bf16[2,2048,512]{2,1,0:T(8,128)(2,1)}) %all-gather.9.cloned.1.call-update) | async-done | bytes 4194320 | tf_op jit(solution)/shard_map/all_gather | solution.py:26
  355.8 0.0 copy-start.3
  355.8 0.0 copy-start.4
  355.8 0.0 copy-start.1
  355.8 5.4 %convolution_convert_fusion.1 = bf16[384,2048]{1,0:T(8,128)(2,1)} fusion(bf16[2,512,2048]{2,1,0:T(8,128)(2,1)} %all-gather.15.cloned.1.call-done, bf16[384,2048]{1,0:T(8,128)(2,1)S(1)} %copy-done.6, bf16[2,2048,512]{2,1,0:T(8,128)(2,1)} %all-gather.9.cloned.1.call-done, f32[386,512]{1,0:T(8,128)S(1)} %maximum_convert_fusion, f32[512]{0:T(512)S(1)} %bitcast.92, ...), kind=kOutput, calls=%fused_computation.1 | convolution fusion | flops 1613168640 | bytes 9705472 | tf_op jit(solution)/shard_map/dot_general | solution.py:44
  361.2 0.0 reduce-scatter.3.cloned.1.call-update
  361.2 0.0 all-gather.17.cloned.1.call-start
  361.3 0.0 copy-done.3
  361.3 0.0 copy-done.4
  361.3 26.6 %reduce-scatter.3.cloned.1.call-done = bf16[384,512]{1,0:T(8,128)(2,1)} async-done(((bf16[384,2048]{1,0:T(8,128)(2,1)}), bf16[384,512]{1,0:T(8,128)(2,1)}) %reduce-scatter.3.cloned.1.call-update) | async-done | bytes 393232 | tf_op jit(solution)/shard_map/reduce_scatter | solution.py:45
  387.9 0.0 copy-done.1
  387.9 1.3 fusion.34
  389.2 5.8 %all-reduce.1 = (f32[384]{0:T(512)S(1)}, f32[384]{0:T(512)S(1)}) all-reduce(f32[384]{0:T(512)S(1)} %get-tuple-element.8, f32[384]{0:T(512)S(1)} %get-tuple-element.7), channel_id=1, replica_groups=mesh['grp'=2,'sp'=4,'tp'=4] {'tp'}, use_global_device_ids=true, to_apply=%region_4.0 | all-reduce | flops 768 | bytes 6144 | tf_op jit(solution)/shard_map/psum | solution.py:49
  395.0 2.0 add_convert_fusion.1
  397.0 0.0 all-gather.17.cloned.1.call-update
  397.0 0.0 reduce-scatter.5.cloned.1.call-start
  397.0 20.3 %all-gather.17.cloned.1.call-done = bf16[384,2048]{1,0:T(8,128)(2,1)} async-done(((bf16[384,512]{1,0:T(8,128)(2,1)}), bf16[384,2048]{1,0:T(8,128)(2,1)}) %all-gather.17.cloned.1.call-update) | async-done | bytes 1572880 | tf_op jit(solution)/shard_map/all_gather | solution.py:32
  417.4 0.0 copy-start.5
  417.4 0.0 copy-start.7
  417.4 3.2 fusion.25
  420.6 0.1 copy-done.5
  420.7 0.5 copy-done.7
  421.2 1.0 fusion.23
  422.2 3.4 collective-permute-start.2
  425.5 1.3 collective-permute-start.3
  426.8 0.0 collective-permute-done.2
  426.9 4.2 collective-permute-done.3
  431.0 0.1 maximum_convert_fusion.1
  431.1 0.0 copy-start
  431.2 5.5 %convolution_convert_fusion = bf16[384,2048]{1,0:T(8,128)(2,1)} fusion(bf16[2,512,2048]{2,1,0:T(8,128)(2,1)} %all-gather.15.cloned.1.call-done, bf16[384,2048]{1,0:T(8,128)(2,1)S(1)} %copy-done.7, bf16[2,2048,512]{2,1,0:T(8,128)(2,1)} %all-gather.9.cloned.1.call-done, f32[386,512]{1,0:T(8,128)S(1)} %maximum_convert_fusion.1, f32[512]{0:T(512)S(1)} %bitcast.89, ...), kind=kOutput, calls=%fused_computation | convolution fusion | flops 1613168640 | bytes 9705472 | tf_op jit(solution)/shard_map/dot_general | solution.py:44
  436.6 0.0 reduce-scatter.5.cloned.1.call-update
  436.7 27.3 %reduce-scatter.5.cloned.1.call-done = bf16[384,512]{1,0:T(8,128)(2,1)} async-done(((bf16[384,2048]{1,0:T(8,128)(2,1)}), bf16[384,512]{1,0:T(8,128)(2,1)}) %reduce-scatter.5.cloned.1.call-update) | async-done | bytes 393232 | tf_op jit(solution)/shard_map/reduce_scatter | solution.py:45
  464.0 0.0 copy-done
  464.0 1.3 fusion.35
  465.2 5.8 %all-reduce = (f32[384]{0:T(512)S(1)}, f32[384]{0:T(512)S(1)}) all-reduce(f32[384]{0:T(512)S(1)} %get-tuple-element.6, f32[384]{0:T(512)S(1)} %get-tuple-element.5), channel_id=1, replica_groups=mesh['grp'=2,'sp'=4,'tp'=4] {'tp'}, use_global_device_ids=true, to_apply=%region_9.0 | all-reduce | flops 768 | bytes 6144 | tf_op jit(solution)/shard_map/psum | solution.py:49
  471.0 2.0 add_convert_fusion
  (8 shorter events, 0.1 us)
Async XLA Ops:
  6.5 24.7 %all-gather.7.cloned.1.call-start = ((), (), s32[]{:S(2)}) async-start(), calls=%async_computation.2 | async-start | bytes 1966080 | tf_op jit(solution)/shard_map/all_gather | solution.py:32
  7.3 2.7 copy-start.2
  7.3 106.4 %all-gather.13.cloned.1.call-start = ((), (), s32[]{:S(2)}) async-start(), calls=%async_computation.5 | async-start | bytes 5242880 | tf_op jit(solution)/shard_map/all_gather | solution.py:28
  8.0 186.4 %all-gather.11.cloned.1.call-start = ((), (), s32[]{:S(2)}) async-start(), calls=%async_computation.4 | async-start | bytes 5242880 | tf_op jit(solution)/shard_map/all_gather | solution.py:27
  8.8 266.4 %all-gather.15.cloned.1.call-start = ((), (), s32[]{:S(2)}) async-start(), calls=%async_computation.6 | async-start | bytes 5242880 | tf_op jit(solution)/shard_map/all_gather | solution.py:29
  9.3 346.5 %all-gather.9.cloned.1.call-start = ((), (), s32[]{:S(2)}) async-start(), calls=%async_computation.3 | async-start | bytes 5242880 | tf_op jit(solution)/shard_map/all_gather | solution.py:26
  9.9 378.0 %reduce-scatter.3.cloned.1.call-start = ((), (), s32[]{:S(2)}) async-start(), calls=%async_computation.7 | async-start | bytes 1966080 | tf_op jit(solution)/shard_map/reduce_scatter | solution.py:45
  31.3 163.2 %copy-start.6 = (bf16[384,2048]{1,0:T(8,128)(2,1)S(1)}, bf16[384,2048]{1,0:T(8,128)(2,1)}, u32[]{:S(2)}) copy-start(bf16[384,2048]{1,0:T(8,128)(2,1)} %all-gather.7.cloned.1.call-done) | copy-start | bytes 4718596
  197.0 2.6 collective-permute-start
  198.3 5.6 %collective-permute-start.1 = (bf16[1,512]{1,0:T(2,128)(2,1)S(1)}, bf16[1,512]{1,0:T(2,128)(2,1)S(1)}, u32[]{:S(2)}, u32[]{:S(2)}) collective-permute-start(bf16[1,512]{1,0:T(2,128)(2,1)S(1)} %get-tuple-element.16), channel_id=1, source_target_pairs={{4,0},{8,4},{12,8},{5,1},{9,5},{13,9},{6,2},{10,6},{14,10},{7,3},{... | collective-permute-start | bytes 3080 | tf_op jit(solution)/shard_map/ppermute | solution.py:17
  355.8 5.5 %copy-start.3 = (f32[2,512]{1,0:T(2,128)S(1)}, f32[2,512]{1,0:T(2,128)}, u32[]{:S(2)}) copy-start(f32[2,512]{1,0:T(2,128)} %param.14) | copy-start | bytes 12292
  355.8 5.5 %copy-start.4 = (f32[2,512]{1,0:T(2,128)S(1)}, f32[2,512]{1,0:T(2,128)}, u32[]{:S(2)}) copy-start(f32[2,512]{1,0:T(2,128)} %param.15) | copy-start | bytes 12292
  355.8 32.1 %copy-start.1 = (bf16[384,512]{1,0:T(8,128)(2,1)S(1)}, bf16[384,512]{1,0:T(8,128)(2,1)}, u32[]{:S(2)}) copy-start(bf16[384,512]{1,0:T(8,128)(2,1)} %param.8) | copy-start | bytes 1179652
  361.2 56.1 %all-gather.17.cloned.1.call-start = ((), (), s32[]{:S(2)}) async-start(), calls=%async_computation.8 | async-start | bytes 1966080 | tf_op jit(solution)/shard_map/all_gather | solution.py:32
  397.0 67.0 %reduce-scatter.5.cloned.1.call-start = ((), (), s32[]{:S(2)}) async-start(), calls=%async_computation.9 | async-start | bytes 1966080 | tf_op jit(solution)/shard_map/reduce_scatter | solution.py:45
  417.4 3.3 copy-start.5
  417.4 3.8 copy-start.7
  422.2 4.7 collective-permute-start.2
  425.5 5.5 %collective-permute-start.3 = (bf16[1,512]{1,0:T(2,128)(2,1)S(1)}, bf16[1,512]{1,0:T(2,128)(2,1)S(1)}, u32[]{:S(2)}, u32[]{:S(2)}) collective-permute-start(bf16[1,512]{1,0:T(2,128)(2,1)S(1)} %get-tuple-element.14), channel_id=1, source_target_pairs={{4,0},{8,4},{12,8},{5,1},{9,5},{13,9},{6,2},{10,6},{14,10},{7,3},{... | collective-permute-start | bytes 3080 | tf_op jit(solution)/shard_map/ppermute | solution.py:17
  431.1 32.8 %copy-start = (bf16[384,512]{1,0:T(8,128)(2,1)S(1)}, bf16[384,512]{1,0:T(8,128)(2,1)}, u32[]{:S(2)}) copy-start(bf16[384,512]{1,0:T(8,128)(2,1)} %add_convert_fusion.1) | copy-start | bytes 1179652
Sparse Core Ops, SparseCore 0:
  8.9 22.3 all-gather.6
  32.8 80.7 all-gather.12
  115.2 79.2 all-gather.10
  195.9 79.2 all-gather.14
  276.6 79.2 all-gather.8
  361.4 26.5 reduce-scatter.2
  397.1 20.2 all-gather.16
  436.8 27.1 reduce-scatter.4
where the time goes:
time: 480 us
  waiting for transfers between devices  419 us (87%)
  matrix products  20.6 us (4%)
  between operations  13.7 us (3%)
  blocking collectives  11.5 us (2%)
  starting transfers between devices  7.54 us (2%)
  other arithmetic  6.74 us (1%)
    all_gather x1, waiting for transfers between devices, shards(): lax.all_gather(value_weight, 'sp', axis=1, tiled=True)  82.3 us
    all_gather x1, waiting for transfers between devices, shards(): lax.all_gather(gate_weight, 'sp', axis=1, tiled=True)  80.7 us
    all_gather x1, waiting for transfers between devices, shards(): lax.all_gather(inner_weight, 'sp', axis=1, tiled=True)  77.8 us
    all_gather x1, waiting for transfers between devices, shards(): lax.all_gather(out_weight, 'sp', axis=2, tiled=True)  71.1 us
    reduce_scatter x2, waiting for transfers between devices, shards(): lax.psum_scatter(terms.astype(jnp.bfloat16), 'tp', scatter_dimension=1, t...  53.9 us
    all_gather x2, waiting for transfers between devices, shards(): whole = lax.all_gather(x, 'tp', axis=1, tiled=True)  41.6 us
    psum x2, blocking collectives, shards(): lax.psum((jnp.sum(total, axis=1), jnp.sum(total * total, axis=1)), 'tp')  11.5 us
    dot_general x2, matrix products, shards(): terms = jnp.dot(gated, full_out[layer], preferred_element_type=jnp.float32)  10.9 us
  transfers between devices with their start and end apart: 12, of which 10 were waited for; matrix products, arithmetic and copies ran while one was open for 1% of the time, Pallas kernels for 0%

commit v1 on v0

v1 whole, which is shorter than its diff:
```python
import functools

import jax
import jax.numpy as jnp
from jax import lax
from jax.experimental import pallas as pl
from jax.experimental.pallas import tpu as pltpu
from jax.sharding import PartitionSpec as P

MESH = pl.DeviceIdType.MESH
F32 = jnp.float32
BF16 = jnp.bfloat16


def extended(value, sides, width):
    for axis, dim in sides:
        peers, length = (lax.axis_size(axis), value.shape[dim])
        up = [(i, (i + 1) % peers) for i in range(peers - 1)]
        down = [(j, i) for i, j in up]
        last = lax.slice_in_dim(value, length - width, length, axis=dim)
        initial = lax.slice_in_dim(value, 0, width, axis=dim)
        before = lax.ppermute(last, axis, up)
        after = lax.ppermute(initial, axis, down)
        value = jnp.concatenate([before, value, after], axis=dim)
    return value


def shards(tokens, gate_weight, inner_weight, value_weight, out_weight, taps, norm_gain, norm_bias):
    x = tokens
    width = x.shape[1] * lax.axis_size("tp")
    full_gate, full_inner, full_value, full_out = (
        lax.all_gather(gate_weight, "sp", axis=1, tiled=True),
        lax.all_gather(inner_weight, "sp", axis=1, tiled=True),
        lax.all_gather(value_weight, "sp", axis=1, tiled=True),
        lax.all_gather(out_weight, "sp", axis=2, tiled=True),
    )
    for layer in range(gate_weight.shape[0]):
        whole = lax.all_gather(x, "tp", axis=1, tiled=True)
        outer = jnp.dot(whole, full_gate[layer], preferred_element_type=F32).astype(BF16)
        inner = jnp.dot(whole, full_inner[layer], preferred_element_type=F32).astype(BF16)
        values = jnp.dot(whole, full_value[layer], preferred_element_type=F32).astype(BF16)
        product = (inner.astype(F32) * values.astype(F32)).astype(BF16)
        padded = extended(product, (("sp", 0),), 1).astype(F32)
        kernel = taps[layer].astype(F32)
        conv = kernel[0] * padded[:-2] + kernel[1] * padded[1:-1] + kernel[2] * padded[2:]
        gated = (outer.astype(F32) * conv).astype(BF16)
        terms = jnp.dot(gated, full_out[layer], preferred_element_type=F32)
        branch = lax.psum_scatter(
            terms.astype(BF16), "tp", scatter_dimension=1, tiled=True
        ).astype(F32)
        total = 2.0**0.5 * x.astype(F32) + branch
        row_sum, row_square = lax.psum(
            (jnp.sum(total, axis=1), jnp.sum(total * total, axis=1)), "tp"
        )
        mean = (row_sum / width)[:, None]
        spread = (row_square / width)[:, None] - mean * mean
        x = (
            (total - mean) * lax.rsqrt(spread + 1e-05) * norm_gain[layer] + norm_bias[layer]
        ).astype(BF16)
    return x


def mixer(layers, x_hbm, wi, wv, wg, wo, taps, gain, bias, out,
          gbuf, xfull, ibuf, pbuf, obuf, gated, tot, halo,
          sib_out, sib_in, far_out, far_in, st_out, st_in,
          s_local, s_x, s_own_r, s_own_l, s_fwd, s_y, r_z, r_y,
          s_halo, r_halo, s_ag, r_ag, s_rs, r_rs, s_st, r_st):
    g, s, t = lax.axis_index("grp"), lax.axis_index("sp"), lax.axis_index("tp")
    weights = (wi, wv, wg, wo)
    rows, chan = x_hbm.shape
    block = chan
    half = block // 2
    width = xfull.shape[2]
    units = 4 * layers
    last = lax.axis_size("sp") - 1
    sib = t + 1 - 2 * lax.rem(t, 2)
    far = lax.rem(t + 2, 4)
    diag = lax.rem(sib + 2, 4)
    own = pl.ds(pl.multiple_of(t * chan, 128), chan)
    grp_peer = 1 - g

    def local(u):
        layer, m = divmod(u, 4)
        return pltpu.make_async_copy(
            weights[m].at[layer],
            gbuf.at[u, pl.ds(pl.multiple_of(s * block, block), block)],
            s_local.at[u])

    x_copy = pltpu.make_async_copy(x_hbm, xfull.at[0, :, own], s_x)
    x_copy.start()
    for u in range(units):
        local(u).start()

    barrier = pltpu.get_barrier_semaphore()

    def hello(dg, ds, dt):
        pl.semaphore_signal(barrier, 1, device_id=(dg, ds, dt), device_id_type=MESH)

    hello(grp_peer, s, t)
    for k in (1, 2, 3):
        hello(g, s, lax.rem(t + k, 4))

    @pl.when(s > 0)
    def _():
        hello(g, s - 1, t)

    @pl.when(s < last)
    def _():
        hello(g, s + 1, t)

    pl.semaphore_wait(barrier, 4 + jnp.where(s > 0, 1, 0) + jnp.where(s < last, 1, 0))

    def piece(u, src, side):
        return gbuf.at[u, pl.ds(pl.multiple_of(src * block + side * half, half), half)]

    def remote(src, dst, send, recv, to):
        return pltpu.make_async_remote_copy(
            src_ref=src, dst_ref=dst, send_sem=send, recv_sem=recv,
            device_id=to, device_id_type=MESH)

    def own_right(u):
        p = piece(u, s, g)
        return remote(p, p, s_own_r.at[u], r_z.at[u, s], (g, s + 1, t))

    def own_left(u):
        p = piece(u, s, g)
        return remote(p, p, s_own_l.at[u], r_z.at[u, s], (g, s - 1, t))

    sources = (
        s + 1 - 2 * lax.rem(s, 2),
        jnp.where(s < 2, 2, 1),
        jnp.where(s < 2, 3, 0),
    )

    def forward(u, k):
        src = sources[k]
        p = piece(u, src, g)
        return remote(p, p, s_fwd.at[u, k], r_z.at[u, src],
                      (g, jnp.where(src > s, s - 1, s + 1), t))

    def across(u, k, side):
        src = sources[k]
        p = piece(u, src, side)
        return remote(p, p, s_y.at[u, k], r_y.at[u, k], (grp_peer, s, t))

    middle = jnp.logical_and(s > 0, s < last)

    def send_own(u):
        local(u).wait()

        @pl.when(s < last)
        def _():
            own_right(u).start()

        @pl.when(s > 0)
        def _():
            own_left(u).start()

    def event(u, k):
        src = sources[k]
        p = piece(u, src, g)
        remote(p, p, s_fwd.at[u, k], r_z.at[u, src], (grp_peer, s, t)).wait_recv()

        @pl.when(middle)
        def _():
            forward(u, k).start()

        across(u, k, g).start()

    def unit_ready(u):
        for k in range(3):
            across(u, k, grp_peer).wait_recv()

    def column(owner):
        return pl.ds(pl.multiple_of(owner * chan, 128), chan)

    def ag(layer, i):
        owner = (t, t, far)[i]
        to = (far, sib, sib)[i]
        ref = xfull.at[layer, :, column(owner)]
        return remote(ref, ref, s_ag.at[layer, i], r_ag.at[layer, i], (g, s, to))

    def ag_recv(layer, i):
        owner = (far, sib, diag)[i]
        ref = xfull.at[layer, :, column(owner)]
        remote(ref, ref, s_ag.at[layer, i], r_ag.at[layer, i], (g, s, sib)).wait_recv()

    def ag_start(layer):
        ag(layer, 0).start()
        ag(layer, 1).start()

    def ag_forward(layer):
        ag_recv(layer, 0)
        ag(layer, 2).start()

    def ag_finish(layer):
        ag_recv(layer, 1)
        ag_recv(layer, 2)

    tile = 256

    def project(layer, m, store):
        u = 4 * layer + m
        unit_ready(u)

        @pl.loop(0, chan // tile)
        def _(n):
            cols = pl.ds(pl.multiple_of(n * tile, tile), tile)
            store(cols, jnp.dot(xfull[layer], gbuf[u, :, cols],
                                preferred_element_type=F32).astype(BF16))

    edge = halo.shape[2]

    def halo_up(layer):
        return remote(pbuf.at[layer, pl.ds(rows - edge, edge)], halo.at[layer, 0],
                      s_halo.at[layer, 0], r_halo.at[layer, 0], (g, s + 1, t))

    def halo_down(layer):
        return remote(pbuf.at[layer, pl.ds(0, edge)], halo.at[layer, 1],
                      s_halo.at[layer, 1], r_halo.at[layer, 1], (g, s - 1, t))

    def do_inner(layer):
        def store(cols, value):
            ibuf[:, cols] = value
        project(layer, 0, store)

    def do_value(layer):
        def store(cols, value):
            pbuf[layer, :, cols] = (ibuf[:, cols].astype(F32) * value.astype(F32)).astype(BF16)
        project(layer, 1, store)

        @pl.when(s < last)
        def _():
            halo_up(layer).start()

        @pl.when(s > 0)
        def _():
            halo_down(layer).start()

    def do_gate(layer):
        def store(cols, value):
            obuf[:, cols] = value
        project(layer, 2, store)

    def do_conv(layer):
        @pl.when(s > 0)
        def _():
            halo_up(layer).wait_recv()

        @pl.when(s < last)
        def _():
            halo_down(layer).wait_recv()

        @pl.loop(0, chan // 128)
        def _(n):
            cols = pl.ds(pl.multiple_of(n * 128, 128), 128)
            p = pbuf[layer, :, cols].astype(F32)
            row = lax.broadcasted_iota(jnp.int32, p.shape, 0)
            first = jnp.where(s > 0, halo[layer, 0, :, cols].astype(F32)[edge - 1:edge], 0.0)
            final = jnp.where(s < last, halo[layer, 1, :, cols].astype(F32)[0:1], 0.0)
            before = jnp.where(row == 0, first, pltpu.roll(p, 1, 0))
            after = jnp.where(row == rows - 1, final, pltpu.roll(p, rows - 1, 0))
            k = taps[layer, :, cols].astype(F32)
            conv = k[0:1] * before + k[1:2] * p + k[2:3] * after
            gated[:, cols] = (obuf[:, cols].astype(F32) * conv).astype(BF16)

    def term(layer, owner, store):
        u = 4 * layer + 3

        @pl.loop(0, chan // tile)
        def _(n):
            cols = pl.ds(pl.multiple_of(n * tile, tile), tile)
            w = gbuf[u, pl.ds(pl.multiple_of(owner * block, block), block), cols]
            store(cols, jnp.dot(gated[...], w, preferred_element_type=F32).astype(BF16))

    def to_sib(layer, i):
        return remote(sib_out.at[layer, i], sib_in.at[layer, i],
                      s_rs.at[layer, i], r_rs.at[layer, i], (g, s, sib))

    def to_far(layer):
        return remote(far_out.at[layer], far_in.at[layer],
                      s_rs.at[layer, 2], r_rs.at[layer, 2], (g, s, far))

    def do_out(layer):
        unit_ready(4 * layer + 3)
        for i, owner in ((0, diag), (1, sib)):
            def store(cols, value):
                sib_out[layer, i, :, cols] = value
            term(layer, owner, store)
            to_sib(layer, i).start()

    def do_far(layer):
        to_sib(layer, 0).wait_recv()

        def store(cols, value):
            far_out[layer, :, cols] = (
                value.astype(F32) + sib_in[layer, 0, :, cols].astype(F32)).astype(BF16)
        term(layer, far, store)
        to_far(layer).start()

    def stat(layer, i):
        return remote(st_out.at[layer], st_in.at[layer, i], s_st.at[layer, i],
                      r_st.at[layer, i], (g, s, (sib, far, diag)[i]))

    def do_total(layer):
        to_sib(layer, 1).wait_recv()

        def store(cols, value):
            mine = pl.ds(pl.multiple_of(t * chan + cols.start, 128), tile)
            tot[:, cols] = (2.0**0.5 * xfull[layer, :, mine].astype(F32) + value.astype(F32)
                            + sib_in[layer, 1, :, cols].astype(F32))
        term(layer, t, store)

    def do_stats(layer):
        to_far(layer).wait_recv()
        total_sum = jnp.zeros((rows, 128), F32)
        total_square = jnp.zeros((rows, 128), F32)
        for n in range(chan // 128):
            cols = slice(n * 128, n * 128 + 128)
            z = tot[:, cols] + far_in[layer, :, cols].astype(F32)
            tot[:, cols] = z
            total_sum = total_sum + z
            total_square = total_square + z * z
        st_out[layer, 0:1, :] = jnp.sum(total_sum.T, axis=0, keepdims=True)
        st_out[layer, 1:2, :] = jnp.sum(total_square.T, axis=0, keepdims=True)
        for i in range(3):
            stat(layer, i).start()

    def do_norm(layer, store):
        for i in range(3):
            stat(layer, i).wait_recv()
        both = st_out[layer] + st_in[layer, 0] + st_in[layer, 1] + st_in[layer, 2]
        mean = both[0:1] / width
        spread = both[1:2] / width - mean * mean
        scale = lax.rsqrt(spread + 1e-05)
        mean = jnp.broadcast_to(mean, (128, rows)).T
        scale = jnp.broadcast_to(scale, (128, rows)).T
        for n in range(chan // 128):
            cols = slice(n * 128, n * 128 + 128)
            z = (tot[:, cols] - mean) * scale * gain[layer:layer + 1, cols] + bias[layer:layer + 1, cols]
            store(n, z.astype(BF16))

    def do_next(layer):
        def store(n, value):
            xfull[layer + 1, :, pl.ds(pl.multiple_of(t * chan + n * 128, 128), 128)] = value
        do_norm(layer, store)
        ag_start(layer + 1)

    def do_result(layer):
        def store(n, value):
            out[:, n * 128:n * 128 + 128] = value
        do_norm(layer, store)

    st_out[...] = jnp.zeros_like(st_out)
    ahead = 2
    for u in range(min(ahead, units)):
        send_own(u)
    x_copy.wait()
    ag_start(0)

    steps = {}

    def put(u, k, step, layer):
        at = min(3 * u + k, 3 * units - 1)
        steps.setdefault(at, []).append((step, layer))

    put(0, 1, ag_forward, 0)
    put(0, 2, ag_finish, 0)
    for layer in range(layers):
        b = 4 * layer
        if layer > 0:
            put(b + 2, 1, ag_forward, layer)
            put(b + 2, 2, ag_finish, layer)
            put(b + 2, 2, do_inner, layer)
            put(b + 3, 0, do_value, layer)
            put(b + 3, 1, do_gate, layer)
        else:
            put(b + 1, 1, do_inner, layer)
            put(b + 2, 1, do_value, layer)
            put(b + 3, 1, do_gate, layer)
        put(b + 3, 2, do_conv, layer)
        put(b + 4, 1, do_out, layer)
        put(b + 4, 2, do_far, layer)
        put(b + 4, 2, do_total, layer)
        put(b + 5, 1, do_stats, layer)
        put(b + 5, 2, do_next if layer < layers - 1 else do_result, layer)

    for u in range(units):
        if u + ahead < units:
            send_own(u + ahead)
        for k in range(3):
            event(u, k)
            for step, layer in steps.get(3 * u + k, ()):
                step(layer)

    for u in range(units):
        @pl.when(s < last)
        def _():
            own_right(u).wait_send()

        @pl.when(s > 0)
        def _():
            own_left(u).wait_send()

        for k in range(3):
            @pl.when(middle)
            def _():
                forward(u, k).wait_send()

            across(u, k, g).wait_send()
    for layer in range(layers):
        @pl.when(s < last)
        def _():
            halo_up(layer).wait_send()

        @pl.when(s > 0)
        def _():
            halo_down(layer).wait_send()

        for i in range(3):
            ag(layer, i).wait_send()
            stat(layer, i).wait_send()
        to_sib(layer, 0).wait_send()
        to_sib(layer, 1).wait_send()
        to_far(layer).wait_send()


def fused(tokens, gate_weight, inner_weight, value_weight, out_weight, taps, norm_gain, norm_bias):
    rows, chan = tokens.shape
    layers = gate_weight.shape[0]
    width = chan * lax.axis_size("tp")
    units = 4 * layers
    dma = pltpu.SemaphoreType.DMA
    hbm = pl.BlockSpec(memory_space=pltpu.HBM)
    vmem = pl.BlockSpec(memory_space=pltpu.VMEM)
    return pl.pallas_call(
        functools.partial(mixer, layers),
        out_shape=jax.ShapeDtypeStruct((rows, chan), BF16),
        in_specs=[hbm] * 5 + [vmem] * 3,
        out_specs=vmem,
        scratch_shapes=[
            pltpu.VMEM((units, width, chan), BF16),
            pltpu.VMEM((layers, rows, width), BF16),
            pltpu.VMEM((rows, chan), BF16),
            pltpu.VMEM((layers, rows, chan), BF16),
            pltpu.VMEM((rows, chan), BF16),
            pltpu.VMEM((rows, chan), BF16),
            pltpu.VMEM((rows, chan), F32),
            pltpu.VMEM((layers, 2, 16, chan), BF16),
            pltpu.VMEM((layers, 2, rows, chan), BF16),
            pltpu.VMEM((layers, 2, rows, chan), BF16),
            pltpu.VMEM((layers, rows, chan), BF16),
            pltpu.VMEM((layers, rows, chan), BF16),
            pltpu.VMEM((layers, 8, rows), F32),
            pltpu.VMEM((layers, 3, 8, rows), F32),
            dma((units,)), dma, dma((units,)), dma((units,)),
            dma((units, 3)), dma((units, 3)), dma((units, 4)), dma((units, 3)),
            dma((layers, 2)), dma((layers, 2)), dma((layers, 3)), dma((layers, 3)),
            dma((layers, 3)), dma((layers, 3)), dma((layers, 3)), dma((layers, 3)),
        ],
        compiler_params=pltpu.CompilerParams(
            collective_id=0, has_side_effects=True, vmem_limit_bytes=48 * 2**20),
    )(tokens, inner_weight, value_weight, gate_weight, out_weight, taps, norm_gain, norm_bias)


def solution(mesh):
    in_specs = (
        P(("grp", "sp"), "tp"),
        P(None, "sp", "tp"),
        P(None, "sp", "tp"),
        P(None, "sp", "tp"),
        P(None, "tp", "sp"),
        P(None, None, "tp"),
        P(None, "tp"),
        P(None, "tp"),
    )
    out_specs = P(("grp", "sp"), "tp")
    routed = (mesh.shape["grp"], mesh.shape["sp"], mesh.shape["tp"]) == (2, 4, 4)
    body = fused if routed else shards
    return jax.shard_map(body, mesh=mesh, in_specs=in_specs, out_specs=out_specs, check_vma=False)
```

time: 480 us -> 186 us (0.39)
  waiting for transfers between devices: 419 us -> 0 us
  Pallas kernels: 0 us -> 178 us
  matrix products: 20.6 us -> 0 us
  between operations: 13.7 us -> 0.03 us
  blocking collectives: 11.5 us -> 0 us
  starting transfers between devices: 7.54 us -> 0 us
  other arithmetic: 6.74 us -> 0 us
  local copies, waits for them, and re-layouts: 0.65 us -> 7.37 us
    all_gather x6 -> x0, waiting for transfers between devices: 354 us -> none  [the longest x1 82.3 us: shards(): lax.all_gather(value_weight, 'sp', axis=1, tiled=True)]
    pallas_call x0 -> x1, Pallas kernels: none -> 178 us  [fused(): pl.pallas_call(functools.partial(mixer, layers), out_shape=jax.ShapeDtype...]
    reduce_scatter x2 -> x0, waiting for transfers between devices: 53.9 us -> none  [shards(): lax.psum_scatter(terms.astype(jnp.bfloat16), 'tp', scatter_dimension=1, t...]
    dot_general x6 -> x0, matrix products: 20.6 us -> none  [the longest x2 10.9 us: shards(): terms = jnp.dot(gated, full_out[layer], preferred_element_type=jnp.float32)]
    psum x2 -> x0, blocking collectives: 11.5 us -> none  [shards(): lax.psum((jnp.sum(total, axis=1), jnp.sum(total * total, axis=1)), 'tp')]
    ppermute x4 -> x0, waiting for transfers between devices: 8.41 us -> none  [the longest x2 8.4 us: extended(): after = lax.ppermute(initial, axis, down)]
    ppermute x4 -> x0, starting transfers between devices: 7.26 us -> none  [the longest x2 4.68 us: extended(): before = lax.ppermute(last, axis, up)]
    unnamed x16, local copies, waits for them, and re-layouts: 0.61 us -> 7.37 us
  transfers between devices with their start and end apart: 12 -> 0, of which waited for: 10 -> 0; matrix products, arithmetic and copies ran while one was open for 1% -> 0% of each run, Pallas kernels for 0% -> 0%
where the time goes in v1:
time: 186 us; the launch traced here: 185 us
  Pallas kernels  178 us (96%)
  local copies, waits for them, and re-layouts  7.37 us (4%)
    pallas_call x1, Pallas kernels, fused(): pl.pallas_call(functools.partial(mixer, layers), out_shape=jax.ShapeDtype...  178 us
    unnamed x16, local copies, waits for them, and re-layouts  7.37 us

profile of v1, /device:TPU:0, one launch (start us, length us, event | category | flops | bytes accessed | tf_op | source)
XLA Modules:
  0.0 185.5 jit_solution(4699754262411007851)
XLA Ops:
  0.0 0.0 copy-start.6
  0.0 0.0 copy-start.5
  0.0 0.7 copy.9.taps
  0.7 0.0 copy-done.6
  0.7 0.0 copy-done.5
  0.7 0.0 copy-start
  0.7 1.2 copy-done
  2.0 0.0 copy-start.1
  2.0 1.2 copy-done.1
  3.2 0.0 copy-start.2
  3.2 1.2 copy-done.2
  4.4 0.0 copy-start.3
  4.4 1.2 copy-done.3
  5.6 0.0 copy-start.4
  5.6 1.0 copy-done.4
  6.6 178.1 %shard_map.82 = bf16[384,512]{1,0:T(8,128)(2,1)S(1)} custom-call(bf16[384,512]{1,0:T(8,128)(2,1)S(1)} %copy-done.4, bf16[2,512,512]{2,1,0:T(8,128)(2,1)S(1)} %copy-done, bf16[2,512,512]{2,1,0:T(8,128)(2,1)S(1)} %copy-done.1, bf16[2,512,512]{2,1,0:T(8,128)(2,1)S(1)} %copy-done.2, bf16[2,512,512]{2,1,0:T(8,128)(2,1)S(1)} %copy-done.3, ...), custom_call_target="tpu_custom_call" | custom-call | tf_op jit(solution)/shard_map/pallas_call | solution.py:436
  184.7 0.7 copy.11
Async XLA Ops:
  0.0 0.7 copy-start.6
  0.0 0.7 copy-start.5
  0.7 1.2 copy-start
  2.0 1.2 copy-start.1
  3.2 1.2 copy-start.2
  4.4 1.2 copy-start.3
  5.6 1.0 copy-start.4

commit v2 on v0

v2 whole, which is shorter than its diff:
```python
import functools

import jax
import jax.numpy as jnp
from jax import lax
from jax.experimental import pallas as pl
from jax.experimental.pallas import tpu as pltpu
from jax.sharding import PartitionSpec as P

MESH = pl.DeviceIdType.MESH
F32 = jnp.float32
BF16 = jnp.bfloat16


def extended(value, sides, width):
    for axis, dim in sides:
        peers, length = (lax.axis_size(axis), value.shape[dim])
        up = [(i, (i + 1) % peers) for i in range(peers - 1)]
        down = [(j, i) for i, j in up]
        last = lax.slice_in_dim(value, length - width, length, axis=dim)
        initial = lax.slice_in_dim(value, 0, width, axis=dim)
        before = lax.ppermute(last, axis, up)
        after = lax.ppermute(initial, axis, down)
        value = jnp.concatenate([before, value, after], axis=dim)
    return value


def shards(tokens, gate_weight, inner_weight, value_weight, out_weight, taps, norm_gain, norm_bias):
    x = tokens
    width = x.shape[1] * lax.axis_size("tp")
    full_gate, full_inner, full_value, full_out = (
        lax.all_gather(gate_weight, "sp", axis=1, tiled=True),
        lax.all_gather(inner_weight, "sp", axis=1, tiled=True),
        lax.all_gather(value_weight, "sp", axis=1, tiled=True),
        lax.all_gather(out_weight, "sp", axis=2, tiled=True),
    )
    for layer in range(gate_weight.shape[0]):
        whole = lax.all_gather(x, "tp", axis=1, tiled=True)
        outer = jnp.dot(whole, full_gate[layer], preferred_element_type=F32).astype(BF16)
        inner = jnp.dot(whole, full_inner[layer], preferred_element_type=F32).astype(BF16)
        values = jnp.dot(whole, full_value[layer], preferred_element_type=F32).astype(BF16)
        product = (inner.astype(F32) * values.astype(F32)).astype(BF16)
        padded = extended(product, (("sp", 0),), 1).astype(F32)
        kernel = taps[layer].astype(F32)
        conv = kernel[0] * padded[:-2] + kernel[1] * padded[1:-1] + kernel[2] * padded[2:]
        gated = (outer.astype(F32) * conv).astype(BF16)
        terms = jnp.dot(gated, full_out[layer], preferred_element_type=F32)
        branch = lax.psum_scatter(
            terms.astype(BF16), "tp", scatter_dimension=1, tiled=True
        ).astype(F32)
        total = 2.0**0.5 * x.astype(F32) + branch
        row_sum, row_square = lax.psum(
            (jnp.sum(total, axis=1), jnp.sum(total * total, axis=1)), "tp"
        )
        mean = (row_sum / width)[:, None]
        spread = (row_square / width)[:, None] - mean * mean
        x = (
            (total - mean) * lax.rsqrt(spread + 1e-05) * norm_gain[layer] + norm_bias[layer]
        ).astype(BF16)
    return x


def mixer(layers, x_hbm, wi, wv, wg, wo, taps, gain, bias, out,
          gbuf, xfull, ibuf, pbuf, obuf, gated, tot, halo, final,
          sib_out, sib_in, far_out, far_in, st_out, st_in,
          s_local, s_x, s_own, s_fwd, s_y, r_z, r_y,
          s_end, r_end, s_tok, r_tok, s_res, r_res,
          s_halo, r_halo, s_ag, r_ag, s_rs, r_rs, s_st, r_st):
    g, s, t = lax.axis_index("grp"), lax.axis_index("sp"), lax.axis_index("tp")
    weights = (wi, wv, wg, wo)
    rows, chan = x_hbm.shape
    block = chan
    half = block // 2
    width = xfull.shape[2]
    units = 4 * layers
    last = lax.axis_size("sp") - 1
    sib = t + 1 - 2 * lax.rem(t, 2)
    far = lax.rem(t + 2, 4)
    diag = lax.rem(sib + 2, 4)
    grp_peer = 1 - g
    is_end = jnp.logical_or(s == 0, s == last)
    is_middle = jnp.logical_and(s > 0, s < last)
    mate = s + 1 - 2 * lax.rem(s, 2)
    inner = last - s
    beyond = last - mate

    def column(owner):
        return pl.ds(pl.multiple_of(owner * chan, 128), chan)

    def token_rows(h):
        holder = mate if h == 0 else s
        return pl.ds(pl.multiple_of(lax.rem(holder, 2) * rows, rows), rows)

    def local(u):
        layer, m = divmod(u, 4)
        return pltpu.make_async_copy(
            weights[m].at[layer],
            gbuf.at[u, pl.ds(pl.multiple_of(s * block, block), block)],
            s_local.at[u])

    x_copy = pltpu.make_async_copy(x_hbm, xfull.at[0, token_rows(1), column(t)], s_x)
    x_copy.start()
    for u in range(units):
        local(u).start()

    barrier = pltpu.get_barrier_semaphore()

    def hello(dg, ds, dt):
        pl.semaphore_signal(barrier, 1, device_id=(dg, ds, dt), device_id_type=MESH)

    hello(g, mate, t)

    @pl.when(is_middle)
    def _():
        hello(grp_peer, s, t)
        hello(g, inner, t)
        for k in (1, 2, 3):
            hello(g, s, lax.rem(t + k, 4))

    pl.semaphore_wait(barrier, jnp.where(is_middle, 6, 1))

    def remote(src, dst, send, recv, to):
        return pltpu.make_async_remote_copy(
            src_ref=src, dst_ref=dst, send_sem=send, recv_sem=recv,
            device_id=to, device_id_type=MESH)

    def piece(u, src, side):
        return gbuf.at[u, pl.ds(pl.multiple_of(src * block + side * half, half), half)]

    def tokens_in():
        ref = xfull.at[0, token_rows(1), column(t)]
        return remote(ref, ref, s_tok, r_tok, (g, mate, t))

    def end_piece(u, i):
        p = piece(u, s, g if i == 0 else 1 - g)
        return remote(p, p, s_end.at[u, i], r_end.at[u, i], (g, mate, t))

    def result():
        return remote(final, out, s_res, r_res, (g, mate, t))

    @pl.when(is_end)
    def _():
        x_copy.wait()
        tokens_in().start()
        for u in range(units):
            local(u).wait()
            if u >= 2:
                end_piece(u - 2, 0).wait_send()
                end_piece(u - 2, 1).wait_send()
            end_piece(u, 0).start()
            end_piece(u, 1).start()
        for u in range(units - 2, units):
            end_piece(u, 0).wait_send()
            end_piece(u, 1).wait_send()
        tokens_in().wait_send()
        result().wait_recv()

    def own_in(u):
        p = piece(u, s, g)
        return remote(p, p, s_own.at[u], r_z.at[u, 0], (g, inner, t))

    def forward(u):
        p = piece(u, mate, g)
        return remote(p, p, s_fwd.at[u], r_z.at[u, 1], (g, inner, t))

    def across(u, k, side):
        p = piece(u, inner if k == 0 else beyond, side)
        return remote(p, p, s_y.at[u, k], r_y.at[u, k], (grp_peer, s, t))

    def event(u, k):
        if k == 0:
            p = piece(u, mate, g)
            remote(p, p, s_end.at[u, 0], r_end.at[u, 0], (g, mate, t)).wait_recv()
            forward(u).start()
        else:
            p = piece(u, inner if k == 1 else beyond, g)
            remote(p, p, s_fwd.at[u], r_z.at[u, k - 1], (g, inner, t)).wait_recv()
            across(u, k - 1, g).start()

    def send_own(u):
        local(u).wait()
        own_in(u).start()

    def unit_ready(u):
        p = piece(u, mate, 1 - g)
        remote(p, p, s_end.at[u, 1], r_end.at[u, 1], (g, mate, t)).wait_recv()
        across(u, 0, grp_peer).wait_recv()
        across(u, 1, grp_peer).wait_recv()

    def ag(layer, h, i):
        owner = (t, t, far)[i]
        to = (far, sib, sib)[i]
        ref = xfull.at[layer, token_rows(h), column(owner)]
        return remote(ref, ref, s_ag.at[layer, h, i], r_ag.at[layer, h, i], (g, s, to))

    def ag_recv(layer, h, i):
        owner = (far, sib, diag)[i]
        ref = xfull.at[layer, token_rows(h), column(owner)]
        remote(ref, ref, s_ag.at[layer, h, i], r_ag.at[layer, h, i], (g, s, sib)).wait_recv()

    def ag_start(layer, h):
        ag(layer, h, 0).start()
        ag(layer, h, 1).start()

    def ag_forward(layer, h):
        ag_recv(layer, h, 0)
        ag(layer, h, 2).start()

    def ag_finish(layer, h):
        ag_recv(layer, h, 1)
        ag_recv(layer, h, 2)

    def adopt():
        ref = xfull.at[0, token_rows(0), column(t)]
        remote(ref, ref, s_tok, r_tok, (g, mate, t)).wait_recv()
        ag_start(0, 0)

    tile = 256
    tiles = chan // tile

    def project(layer, m, store):
        u = 4 * layer + m
        unit_ready(u)

        @pl.loop(0, 2 * tiles)
        def _(n):
            cols = pl.ds(pl.multiple_of(lax.rem(n, tiles) * tile, tile), tile)
            at = pl.ds(pl.multiple_of((n // tiles) * rows, rows), rows)
            store(at, cols, jnp.dot(xfull[layer, at, :], gbuf[u, :, cols],
                                    preferred_element_type=F32).astype(BF16))

    edge = halo.shape[1]

    def halo_copy(layer):
        edge_row = jnp.where(s < inner, 2 * rows - edge, 0)
        return remote(pbuf.at[layer, pl.ds(pl.multiple_of(edge_row, edge), edge)], halo.at[layer],
                      s_halo.at[layer], r_halo.at[layer], (g, inner, t))

    def do_inner(layer):
        def store(at, cols, value):
            ibuf[at, cols] = value
        project(layer, 0, store)

    def do_value(layer):
        def store(at, cols, value):
            pbuf[layer, at, cols] = (ibuf[at, cols].astype(F32) * value.astype(F32)).astype(BF16)
        project(layer, 1, store)
        halo_copy(layer).start()

    def do_gate(layer):
        def store(at, cols, value):
            obuf[at, cols] = value
        project(layer, 2, store)

    def do_conv(layer):
        halo_copy(layer).wait_recv()

        @pl.loop(0, chan // 128)
        def _(n):
            cols = pl.ds(pl.multiple_of(n * 128, 128), 128)
            p = pbuf[layer, :, cols].astype(F32)
            row = lax.broadcasted_iota(jnp.int32, p.shape, 0)
            met = halo[layer, :, cols].astype(F32)
            first = jnp.where(s > inner, met[edge - 1:edge], 0.0)
            closing = jnp.where(s < inner, met[0:1], 0.0)
            before = jnp.where(row == 0, first, pltpu.roll(p, 1, 0))
            after = jnp.where(row == 2 * rows - 1, closing, pltpu.roll(p, 2 * rows - 1, 0))
            k = taps[layer, :, cols].astype(F32)
            conv = k[0:1] * before + k[1:2] * p + k[2:3] * after
            gated[:, cols] = (obuf[:, cols].astype(F32) * conv).astype(BF16)

    def term(layer, h, owner, store):
        u = 4 * layer + 3
        at = token_rows(h)

        @pl.loop(0, tiles)
        def _(n):
            cols = pl.ds(pl.multiple_of(n * tile, tile), tile)
            w = gbuf[u, pl.ds(pl.multiple_of(owner * block, block), block), cols]
            store(cols, jnp.dot(gated[at, :], w, preferred_element_type=F32).astype(BF16))

    def to_sib(layer, h, i):
        return remote(sib_out.at[layer, h, i], sib_in.at[layer, h, i],
                      s_rs.at[layer, h, i], r_rs.at[layer, h, i], (g, s, sib))

    def to_far(layer, h):
        return remote(far_out.at[layer, h], far_in.at[layer, h],
                      s_rs.at[layer, h, 2], r_rs.at[layer, h, 2], (g, s, far))

    def do_diag(layer, h):
        def store(cols, value):
            sib_out[layer, h, 0, :, cols] = value
        term(layer, h, diag, store)
        to_sib(layer, h, 0).start()

    def do_sib(layer, h):
        def store(cols, value):
            sib_out[layer, h, 1, :, cols] = value
        term(layer, h, sib, store)
        to_sib(layer, h, 1).start()

    def do_far(layer, h):
        to_sib(layer, h, 0).wait_recv()

        def store(cols, value):
            far_out[layer, h, :, cols] = (
                value.astype(F32) + sib_in[layer, h, 0, :, cols].astype(F32)).astype(BF16)
        term(layer, h, far, store)
        to_far(layer, h).start()

    def do_out(layer):
        unit_ready(4 * layer + 3)
        do_diag(layer, 0)
        do_diag(layer, 1)
        do_far(layer, 0)
        do_far(layer, 1)
        do_sib(layer, 0)
        do_sib(layer, 1)
        do_total(layer, 0)
        do_total(layer, 1)

    def stat(layer, h, i):
        return remote(st_out.at[layer, h], st_in.at[layer, h, i], s_st.at[layer, h, i],
                      r_st.at[layer, h, i], (g, s, (sib, far, diag)[i]))

    def do_total(layer, h):
        to_sib(layer, h, 1).wait_recv()
        at = token_rows(h)

        def store(cols, value):
            mine = pl.ds(pl.multiple_of(t * chan + cols.start, 128), tile)
            tot[h, :, cols] = (2.0**0.5 * xfull[layer, at, mine].astype(F32) + value.astype(F32)
                               + sib_in[layer, h, 1, :, cols].astype(F32))
        term(layer, h, t, store)

    def do_stats(layer, h):
        to_far(layer, h).wait_recv()
        total_sum = jnp.zeros((rows, 128), F32)
        total_square = jnp.zeros((rows, 128), F32)
        for n in range(chan // 128):
            cols = slice(n * 128, n * 128 + 128)
            z = tot[h, :, cols] + far_in[layer, h, :, cols].astype(F32)
            tot[h, :, cols] = z
            total_sum = total_sum + z
            total_square = total_square + z * z
        st_out[layer, h, 0:1, :] = jnp.sum(total_sum.T, axis=0, keepdims=True)
        st_out[layer, h, 1:2, :] = jnp.sum(total_square.T, axis=0, keepdims=True)
        for i in range(3):
            stat(layer, h, i).start()

    def do_norm(layer, h, store):
        for i in range(3):
            stat(layer, h, i).wait_recv()
        both = st_out[layer, h] + st_in[layer, h, 0] + st_in[layer, h, 1] + st_in[layer, h, 2]
        mean = both[0:1] / width
        spread = both[1:2] / width - mean * mean
        scale = lax.rsqrt(spread + 1e-05)
        mean = jnp.broadcast_to(mean, (128, rows)).T
        scale = jnp.broadcast_to(scale, (128, rows)).T
        for n in range(chan // 128):
            cols = slice(n * 128, n * 128 + 128)
            z = (tot[h, :, cols] - mean) * scale * gain[layer:layer + 1, cols] + bias[layer:layer + 1, cols]
            store(n, z.astype(BF16))

    def do_next(layer, h):
        at = token_rows(h)

        def store(n, value):
            xfull[layer + 1, at, pl.ds(pl.multiple_of(t * chan + n * 128, 128), 128)] = value
        do_norm(layer, h, store)
        ag_start(layer + 1, h)

    def do_result(layer, h):
        target = final if h == 0 else out

        def store(n, value):
            target[:, n * 128:n * 128 + 128] = value
        do_norm(layer, h, store)
        if h == 0:
            result().start()

    steps = {}

    def put(u, k, step, *args):
        at = min(3 * u + k, 3 * units - 1)
        steps.setdefault(at, []).append((step, args))

    put(0, 0, adopt)
    put(0, 1, ag_forward, 0, 1)
    put(1, 0, ag_forward, 0, 0)
    put(1, 0, ag_finish, 0, 1)
    put(1, 1, ag_finish, 0, 0)
    for layer in range(layers):
        b = 4 * layer
        if layer > 0:
            put(b + 3, 0, ag_forward, layer, 0)
            put(b + 3, 2, ag_forward, layer, 1)
            put(b + 3, 2, ag_finish, layer, 0)
            put(b + 3, 2, ag_finish, layer, 1)
        late = 0 if layer == 0 else 2
        put(b + 1 + late, 1 + late, do_inner, layer)
        put(b + 2 + late, 1, do_value, layer)
        put(b + 3 + late, 1, do_gate, layer)
        put(b + 3 + late, 2, do_conv, layer)
        put(b + 4 + late, 1, do_out, layer)
        after = do_next if layer < layers - 1 else do_result
        put(b + 5 + late, 1, do_stats, layer, 0)
        put(b + 5 + late, 2, after, layer, 0)
        put(b + 6 + late, 0, do_stats, layer, 1)
        put(b + 6 + late, 1, after, layer, 1)

    @pl.when(is_middle)
    def _():
        st_out[...] = jnp.zeros_like(st_out)
        ahead = 2
        for u in range(min(ahead, units)):
            send_own(u)
        x_copy.wait()
        ag_start(0, 1)
        for u in range(units):
            if u + ahead < units:
                send_own(u + ahead)
            for k in range(3):
                event(u, k)
                for step, args in steps.get(3 * u + k, ()):
                    step(*args)

        for u in range(units):
            own_in(u).wait_send()
            forward(u).wait_send()
            across(u, 0, g).wait_send()
            across(u, 1, g).wait_send()
        for layer in range(layers):
            halo_copy(layer).wait_send()
            for h in range(2):
                for i in range(3):
                    ag(layer, h, i).wait_send()
                    stat(layer, h, i).wait_send()
                to_sib(layer, h, 0).wait_send()
                to_sib(layer, h, 1).wait_send()
                to_far(layer, h).wait_send()
        result().wait_send()


def fused(tokens, gate_weight, inner_weight, value_weight, out_weight, taps, norm_gain, norm_bias):
    rows, chan = tokens.shape
    layers = gate_weight.shape[0]
    width = chan * lax.axis_size("tp")
    units = 4 * layers
    dma = pltpu.SemaphoreType.DMA
    hbm = pl.BlockSpec(memory_space=pltpu.HBM)
    vmem = pl.BlockSpec(memory_space=pltpu.VMEM)
    return pl.pallas_call(
        functools.partial(mixer, layers),
        out_shape=jax.ShapeDtypeStruct((rows, chan), BF16),
        in_specs=[hbm] * 5 + [vmem] * 3,
        out_specs=vmem,
        scratch_shapes=[
            pltpu.VMEM((units, width, chan), BF16),
            pltpu.VMEM((layers, 2 * rows, width), BF16),
            pltpu.VMEM((2 * rows, chan), BF16),
            pltpu.VMEM((layers, 2 * rows, chan), BF16),
            pltpu.VMEM((2 * rows, chan), BF16),
            pltpu.VMEM((2 * rows, chan), BF16),
            pltpu.VMEM((2, rows, chan), F32),
            pltpu.VMEM((layers, 16, chan), BF16),
            pltpu.VMEM((rows, chan), BF16),
            pltpu.VMEM((layers, 2, 2, rows, chan), BF16),
            pltpu.VMEM((layers, 2, 2, rows, chan), BF16),
            pltpu.VMEM((layers, 2, rows, chan), BF16),
            pltpu.VMEM((layers, 2, rows, chan), BF16),
            pltpu.VMEM((layers, 2, 8, rows), F32),
            pltpu.VMEM((layers, 2, 3, 8, rows), F32),
            dma((units,)), dma, dma((units,)), dma((units,)),
            dma((units, 2)), dma((units, 2)), dma((units, 2)),
            dma((units, 2)), dma((units, 2)), dma, dma, dma, dma,
            dma((layers,)), dma((layers,)), dma((layers, 2, 3)), dma((layers, 2, 3)),
            dma((layers, 2, 3)), dma((layers, 2, 3)), dma((layers, 2, 3)), dma((layers, 2, 3)),
        ],
        compiler_params=pltpu.CompilerParams(
            collective_id=0, has_side_effects=True, vmem_limit_bytes=58 * 2**20),
    )(tokens, inner_weight, value_weight, gate_weight, out_weight, taps, norm_gain, norm_bias)


def solution(mesh):
    in_specs = (
        P(("grp", "sp"), "tp"),
        P(None, "sp", "tp"),
        P(None, "sp", "tp"),
        P(None, "sp", "tp"),
        P(None, "tp", "sp"),
        P(None, None, "tp"),
        P(None, "tp"),
        P(None, "tp"),
    )
    out_specs = P(("grp", "sp"), "tp")
    routed = (mesh.shape["grp"], mesh.shape["sp"], mesh.shape["tp"]) == (2, 4, 4)
    body = fused if routed else shards
    return jax.shard_map(body, mesh=mesh, in_specs=in_specs, out_specs=out_specs, check_vma=False)
```

time: 480 us -> 164 us (0.34)
  waiting for transfers between devices: 419 us -> 0 us
  Pallas kernels: 0 us -> 160 us
  matrix products: 20.6 us -> 0 us
  between operations: 13.7 us -> 0.01 us
  blocking collectives: 11.5 us -> 0 us
  starting transfers between devices: 7.54 us -> 0 us
  other arithmetic: 6.74 us -> 0 us
    all_gather x6 -> x0, waiting for transfers between devices: 354 us -> none  [the longest x1 82.3 us: shards(): lax.all_gather(value_weight, 'sp', axis=1, tiled=True)]
    pallas_call x0 -> x1, Pallas kernels: none -> 160 us  [fused(): pl.pallas_call(functools.partial(mixer, layers), out_shape=jax.ShapeDtype...]
    reduce_scatter x2 -> x0, waiting for transfers between devices: 53.9 us -> none  [shards(): lax.psum_scatter(terms.astype(jnp.bfloat16), 'tp', scatter_dimension=1, t...]
    dot_general x6 -> x0, matrix products: 20.6 us -> none  [the longest x2 10.9 us: shards(): terms = jnp.dot(gated, full_out[layer], preferred_element_type=jnp.float32)]
    psum x2 -> x0, blocking collectives: 11.5 us -> none  [shards(): lax.psum((jnp.sum(total, axis=1), jnp.sum(total * total, axis=1)), 'tp')]
    ppermute x4 -> x0, waiting for transfers between devices: 8.41 us -> none  [the longest x2 8.4 us: extended(): after = lax.ppermute(initial, axis, down)]
    ppermute x4 -> x0, starting transfers between devices: 7.26 us -> none  [the longest x2 4.68 us: extended(): before = lax.ppermute(last, axis, up)]
  transfers between devices with their start and end apart: 12 -> 0, of which waited for: 10 -> 0; matrix products, arithmetic and copies ran while one was open for 1% -> 0% of each run, Pallas kernels for 0% -> 0%
where the time goes in v2:
time: 164 us
  Pallas kernels  160 us (98%)
  local copies, waits for them, and re-layouts  3.06 us (2%)
    pallas_call x1, Pallas kernels, fused(): pl.pallas_call(functools.partial(mixer, layers), out_shape=jax.ShapeDtype...  160 us

profile of v2, /device:TPU:0, one launch (start us, length us, event | category | flops | bytes accessed | tf_op | source)
XLA Modules:
  0.0 163.5 jit_solution(266397474772614515)
XLA Ops:
  0.0 1.3 copy.9.taps
  1.3 160.4 %shard_map.82 = bf16[384,512]{1,0:T(8,128)(2,1)} custom-call(bf16[384,512]{1,0:T(8,128)(2,1)} %x_hbm.1, bf16[2,512,512]{2,1,0:T(8,128)(2,1)} %wi.1, bf16[2,512,512]{2,1,0:T(8,128)(2,1)} %wv.1, bf16[2,512,512]{2,1,0:T(8,128)(2,1)} %wg.1, bf16[2,512,512]{2,1,0:T(8,128)(2,1)} %wo.1, bf16[2,3,512]{2,1,0:T(4,128)(2,1)} %copy.9.taps, f32[2,512]{1,0:T(2,128)} %gain.1, ...), custom_call_target="tpu_custom_call" | custom-call | tf_op jit(solution)/shard_map/pallas_call | solution.py:453
  161.7 1.8 %copy.11 = bf16[384,512]{1,0:T(8,128)(2,1)} copy(bf16[384,512]{1,0:T(8,128)(2,1)} %shard_map.82) | data formatting | bytes 786432

commit v3 on v2

--- a/solution.py
+++ b/solution.py
@@ -65,7 +65,7 @@
           sib_out, sib_in, far_out, far_in, st_out, st_in,
           s_local, s_x, s_own, s_fwd, s_y, r_z, r_y,
           s_end, r_end, s_tok, r_tok, s_res, r_res,
-          s_halo, r_halo, s_ag, r_ag, s_rs, r_rs, s_st, r_st):
+          s_halo, r_halo, s_ag, r_ag, s_rs, r_rs, s_far, r_far, s_st, r_st):
     g, s, t = lax.axis_index("grp"), lax.axis_index("sp"), lax.axis_index("tp")
     weights = (wi, wv, wg, wo)
     rows, chan = x_hbm.shape
@@ -91,6 +91,18 @@
         holder = mate if h == 0 else s
         return pl.ds(pl.multiple_of(lax.rem(holder, 2) * rows, rows), rows)
 
+    step_rows = 128
+    per_block = rows // step_rows
+    chunks = 2 * per_block
+
+    def inside(c):
+        return pl.ds((c % per_block) * step_rows, step_rows)
+
+    def chunk_rows(c):
+        holder = mate if c < per_block else s
+        start = lax.rem(holder, 2) * rows + (c % per_block) * step_rows
+        return pl.ds(pl.multiple_of(start, step_rows), step_rows)
+
     def local(u):
         layer, m = divmod(u, 4)
         return pltpu.make_async_copy(
@@ -135,25 +147,28 @@
         p = piece(u, s, g if i == 0 else 1 - g)
         return remote(p, p, s_end.at[u, i], r_end.at[u, i], (g, mate, t))
 
-    def result():
-        return remote(final, out, s_res, r_res, (g, mate, t))
+    def result(c):
+        return remote(final.at[inside(c)], out.at[inside(c)], s_res.at[c], r_res.at[c], (g, mate, t))
 
     @pl.when(is_end)
     def _():
         x_copy.wait()
         tokens_in().start()
+        order = [(0, 0)]
+        for u in range(1, units):
+            order += [(u, 0), (u - 1, 1)]
+        order += [(units - 1, 1)]
         for u in range(units):
             local(u).wait()
-            if u >= 2:
-                end_piece(u - 2, 0).wait_send()
-                end_piece(u - 2, 1).wait_send()
-            end_piece(u, 0).start()
-            end_piece(u, 1).start()
-        for u in range(units - 2, units):
-            end_piece(u, 0).wait_send()
-            end_piece(u, 1).wait_send()
+        for n, (u, i) in enumerate(order):
+            if n >= 3:
+                end_piece(*order[n - 3]).wait_send()
+            end_piece(u, i).start()
+        for u, i in order[-3:]:
+            end_piece(u, i).wait_send()
         tokens_in().wait_send()
-        result().wait_recv()
+        for c in range(per_block):
+            result(c).wait_recv()
 
     def own_in(u):
         p = piece(u, s, g)
@@ -187,33 +202,34 @@
         across(u, 0, grp_peer).wait_recv()
         across(u, 1, grp_peer).wait_recv()
 
-    def ag(layer, h, i):
+    def ag(layer, c, i):
         owner = (t, t, far)[i]
         to = (far, sib, sib)[i]
-        ref = xfull.at[layer, token_rows(h), column(owner)]
-        return remote(ref, ref, s_ag.at[layer, h, i], r_ag.at[layer, h, i], (g, s, to))
-
-    def ag_recv(layer, h, i):
+        ref = xfull.at[layer, chunk_rows(c), column(owner)]
+        return remote(ref, ref, s_ag.at[layer, c, i], r_ag.at[layer, c, i], (g, s, to))
+
+    def ag_recv(layer, c, i):
         owner = (far, sib, diag)[i]
-        ref = xfull.at[layer, token_rows(h), column(owner)]
-        remote(ref, ref, s_ag.at[layer, h, i], r_ag.at[layer, h, i], (g, s, sib)).wait_recv()
-
-    def ag_start(layer, h):
-        ag(layer, h, 0).start()
-        ag(layer, h, 1).start()
-
-    def ag_forward(layer, h):
-        ag_recv(layer, h, 0)
-        ag(layer, h, 2).start()
-
-    def ag_finish(layer, h):
-        ag_recv(layer, h, 1)
-        ag_recv(layer, h, 2)
+        ref = xfull.at[layer, chunk_rows(c), column(owner)]
+        remote(ref, ref, s_ag.at[layer, c, i], r_ag.at[layer, c, i], (g, s, sib)).wait_recv()
+
+    def ag_start(layer, c):
+        ag(layer, c, 0).start()
+        ag(layer, c, 1).start()
+
+    def ag_forward(layer, c):
+        ag_recv(layer, c, 0)
+        ag(layer, c, 2).start()
+
+    def ag_finish(layer, c):
+        ag_recv(layer, c, 1)
+        ag_recv(layer, c, 2)
 
     def adopt():
         ref = xfull.at[0, token_rows(0), column(t)]
         remote(ref, ref, s_tok, r_tok, (g, mate, t)).wait_recv()
-        ag_start(0, 0)
+        for c in range(per_block):
+            ag_start(0, c)
 
     tile = 256
     tiles = chan // tile
@@ -283,9 +299,10 @@
         return remote(sib_out.at[layer, h, i], sib_in.at[layer, h, i],
                       s_rs.at[layer, h, i], r_rs.at[layer, h, i], (g, s, sib))
 
-    def to_far(layer, h):
-        return remote(far_out.at[layer, h], far_in.at[layer, h],
-                      s_rs.at[layer, h, 2], r_rs.at[layer, h, 2], (g, s, far))
+    def to_far(layer, c):
+        h = c // per_block
+        return remote(far_out.at[layer, h, inside(c)], far_in.at[layer, h, inside(c)],
+                      s_far.at[layer, c], r_far.at[layer, c], (g, s, far))
 
     def do_diag(layer, h):
         def store(cols, value):
@@ -306,22 +323,23 @@
             far_out[layer, h, :, cols] = (
                 value.astype(F32) + sib_in[layer, h, 0, :, cols].astype(F32)).astype(BF16)
         term(layer, h, far, store)
-        to_far(layer, h).start()
 
     def do_out(layer):
         unit_ready(4 * layer + 3)
         do_diag(layer, 0)
         do_diag(layer, 1)
         do_far(layer, 0)
+        to_far(layer, 0).start()
+        to_far(layer, 1).start()
+        do_sib(layer, 0)
         do_far(layer, 1)
-        do_sib(layer, 0)
         do_sib(layer, 1)
         do_total(layer, 0)
         do_total(layer, 1)
 
-    def stat(layer, h, i):
-        return remote(st_out.at[layer, h], st_in.at[layer, h, i], s_st.at[layer, h, i],
-                      r_st.at[layer, h, i], (g, s, (sib, far, diag)[i]))
+    def stat(layer, c, i):
+        return remote(st_out.at[layer, c], st_in.at[layer, c, i], s_st.at[layer, c, i],
+                      r_st.at[layer, c, i], (g, s, (sib, far, diag)[i]))
 
     def do_total(layer, h):
         to_sib(layer, h, 1).wait_recv()
@@ -333,51 +351,55 @@
                                + sib_in[layer, h, 1, :, cols].astype(F32))
         term(layer, h, t, store)
 
-    def do_stats(layer, h):
-        to_far(layer, h).wait_recv()
-        total_sum = jnp.zeros((rows, 128), F32)
-        total_square = jnp.zeros((rows, 128), F32)
+    def do_stats(layer, c):
+        to_far(layer, c).wait_recv()
+        h, at = c // per_block, inside(c)
+        total_sum = jnp.zeros((step_rows, 128), F32)
+        total_square = jnp.zeros((step_rows, 128), F32)
         for n in range(chan // 128):
             cols = slice(n * 128, n * 128 + 128)
-            z = tot[h, :, cols] + far_in[layer, h, :, cols].astype(F32)
-            tot[h, :, cols] = z
+            z = tot[h, at, cols] + far_in[layer, h, at, cols].astype(F32)
+            tot[h, at, cols] = z
             total_sum = total_sum + z
             total_square = total_square + z * z
-        st_out[layer, h, 0:1, :] = jnp.sum(total_sum.T, axis=0, keepdims=True)
-        st_out[layer, h, 1:2, :] = jnp.sum(total_square.T, axis=0, keepdims=True)
+        st_out[layer, c, 0:1, :] = jnp.sum(total_sum.T, axis=0, keepdims=True)
+        st_out[layer, c, 1:2, :] = jnp.sum(total_square.T, axis=0, keepdims=True)
+        for i in (1, 2, 0):
+            stat(layer, c, i).start()
+
+    def do_norm(layer, c):
         for i in range(3):
-            stat(layer, h, i).start()
-
-    def do_norm(layer, h, store):
-        for i in range(3):
-            stat(layer, h, i).wait_recv()
-        both = st_out[layer, h] + st_in[layer, h, 0] + st_in[layer, h, 1] + st_in[layer, h, 2]
+            stat(layer, c, i).wait_recv()
+        h, at = c // per_block, inside(c)
+        both = st_out[layer, c] + st_in[layer, c, 0] + st_in[layer, c, 1] + st_in[layer, c, 2]
         mean = both[0:1] / width
         spread = both[1:2] / width - mean * mean
         scale = lax.rsqrt(spread + 1e-05)
-        mean = jnp.broadcast_to(mean, (128, rows)).T
-        scale = jnp.broadcast_to(scale, (128, rows)).T
+        mean = jnp.broadcast_to(mean, (step_rows, step_rows)).T
+        scale = jnp.broadcast_to(scale, (step_rows, step_rows)).T
         for n in range(chan // 128):
             cols = slice(n * 128, n * 128 + 128)
-            z = (tot[h, :, cols] - mean) * scale * gain[layer:layer + 1, cols] + bias[layer:layer + 1, cols]
-            store(n, z.astype(BF16))
-
-    def do_next(layer, h):
-        at = token_rows(h)
-
-        def store(n, value):
-            xfull[layer + 1, at, pl.ds(pl.multiple_of(t * chan + n * 128, 128), 128)] = value
-        do_norm(layer, h, store)
-        ag_start(layer + 1, h)
-
-    def do_result(layer, h):
-        target = final if h == 0 else out
-
-        def store(n, value):
-            target[:, n * 128:n * 128 + 128] = value
-        do_norm(layer, h, store)
-        if h == 0:
-            result().start()
+            z = (tot[h, at, cols] - mean) * scale * gain[layer:layer + 1, cols] + bias[layer:layer + 1, cols]
+            value = z.astype(BF16)
+            if layer < layers - 1:
+                to = pl.ds(pl.multiple_of(t * chan + n * 128, 128), 128)
+                xfull[layer + 1, chunk_rows(c), to] = value
+            elif h == 0:
+                final[at, cols] = value
+            else:
+                out[at, cols] = value
+        if layer < layers - 1:
+            ag_start(layer + 1, c)
+        elif h == 0:
+            result(c).start()
+
+    def do_chunk(layer, c):
+        if c < chunks:
+            do_stats(layer, c)
+            if c + 2 < chunks:
+                to_far(layer, c + 2).start()
+        if c > 0:
+            do_norm(layer, c - 1)
 
     steps = {}
 
@@ -386,28 +408,30 @@
         steps.setdefault(at, []).append((step, args))
 
     put(0, 0, adopt)
-    put(0, 1, ag_forward, 0, 1)
-    put(1, 0, ag_forward, 0, 0)
-    put(1, 0, ag_finish, 0, 1)
-    put(1, 1, ag_finish, 0, 0)
+    for c in range(per_block):
+        put(0, 1, ag_forward, 0, per_block + c)
+        put(1, 0, ag_forward, 0, c)
+    for c in range(chunks):
+        put(1, 1, ag_finish, 0, c)
     for layer in range(layers):
         b = 4 * layer
         if layer > 0:
-            put(b + 3, 0, ag_forward, layer, 0)
-            put(b + 3, 2, ag_forward, layer, 1)
-            put(b + 3, 2, ag_finish, layer, 0)
-            put(b + 3, 2, ag_finish, layer, 1)
-        late = 0 if layer == 0 else 2
-        put(b + 1 + late, 1 + late, do_inner, layer)
-        put(b + 2 + late, 1, do_value, layer)
-        put(b + 3 + late, 1, do_gate, layer)
-        put(b + 3 + late, 2, do_conv, layer)
-        put(b + 4 + late, 1, do_out, layer)
-        after = do_next if layer < layers - 1 else do_result
-        put(b + 5 + late, 1, do_stats, layer, 0)
-        put(b + 5 + late, 2, after, layer, 0)
-        put(b + 6 + late, 0, do_stats, layer, 1)
-        put(b + 6 + late, 1, after, layer, 1)
+            for c in range(chunks):
+                put(b + 2, 1 + c // per_block, ag_forward, layer, c)
+            for c in range(chunks):
+                put(b + 3, 0, ag_finish, layer, c)
+            put(b + 3, 0, do_inner, layer)
+            put(b + 3, 1, do_value, layer)
+            put(b + 3, 2, do_gate, layer)
+        else:
+            put(b + 1, 1, do_inner, layer)
+            put(b + 2, 1, do_value, layer)
+            put(b + 3, 1, do_gate, layer)
+        put(b + 3, 2, do_conv, layer)
+        put(b + 4, 1, do_out, layer)
+        for c in range(chunks + 1):
+            k = 3 * (b + 4) + 2 + c * 5 // chunks
+            put(k // 3, k % 3, do_chunk, layer, c)
 
     @pl.when(is_middle)
     def _():
@@ -416,7 +440,8 @@
         for u in range(min(ahead, units)):
             send_own(u)
         x_copy.wait()
-        ag_start(0, 1)
+        for c in range(per_block, chunks):
+            ag_start(0, c)
         for u in range(units):
             if u + ahead < units:
                 send_own(u + ahead)
@@ -432,14 +457,16 @@
             across(u, 1, g).wait_send()
         for layer in range(layers):
             halo_copy(layer).wait_send()
+            for c in range(chunks):
+                for i in range(3):
+                    ag(layer, c, i).wait_send()
+                    stat(layer, c, i).wait_send()
+                to_far(layer, c).wait_send()
             for h in range(2):
-                for i in range(3):
-                    ag(layer, h, i).wait_send()
-                    stat(layer, h, i).wait_send()
                 to_sib(layer, h, 0).wait_send()
                 to_sib(layer, h, 1).wait_send()
-                to_far(layer, h).wait_send()
-        result().wait_send()
+        for c in range(per_block):
+            result(c).wait_send()
 
 
 def fused(tokens, gate_weight, inner_weight, value_weight, out_weight, taps, norm_gain, norm_bias):
@@ -447,6 +474,7 @@
     layers = gate_weight.shape[0]
     width = chan * lax.axis_size("tp")
     units = 4 * layers
+    chunks = 2 * (rows // 128)
     dma = pltpu.SemaphoreType.DMA
     hbm = pl.BlockSpec(memory_space=pltpu.HBM)
     vmem = pl.BlockSpec(memory_space=pltpu.VMEM)
@@ -469,13 +497,14 @@
             pltpu.VMEM((layers, 2, 2, rows, chan), BF16),
             pltpu.VMEM((layers, 2, rows, chan), BF16),
             pltpu.VMEM((layers, 2, rows, chan), BF16),
-            pltpu.VMEM((layers, 2, 8, rows), F32),
-            pltpu.VMEM((layers, 2, 3, 8, rows), F32),
+            pltpu.VMEM((layers, chunks, 8, 128), F32),
+            pltpu.VMEM((layers, chunks, 3, 8, 128), F32),
             dma((units,)), dma, dma((units,)), dma((units,)),
             dma((units, 2)), dma((units, 2)), dma((units, 2)),
-            dma((units, 2)), dma((units, 2)), dma, dma, dma, dma,
-            dma((layers,)), dma((layers,)), dma((layers, 2, 3)), dma((layers, 2, 3)),
-            dma((layers, 2, 3)), dma((layers, 2, 3)), dma((layers, 2, 3)), dma((layers, 2, 3)),
+            dma((units, 2)), dma((units, 2)), dma, dma, dma((chunks,)), dma((chunks,)),
+            dma((layers,)), dma((layers,)), dma((layers, chunks, 3)), dma((layers, chunks, 3)),
+            dma((layers, 2, 2)), dma((layers, 2, 2)), dma((layers, chunks)), dma((layers, chunks)),
+            dma((layers, chunks, 3)), dma((layers, chunks, 3)),
         ],
         compiler_params=pltpu.CompilerParams(
             collective_id=0, has_side_effects=True, vmem_limit_bytes=58 * 2**20),

time: 164 us -> 158 us (0.963); the launches traced: 164 us -> 156 us
  Pallas kernels: 160 us -> 153 us
    pallas_call x1, Pallas kernels: 160 us -> 153 us  [fused(): pl.pallas_call(functools.partial(mixer, layers), out_shape=jax.ShapeDtype...]
where the time goes in v3:
time: 158 us; the launch traced here: 156 us
  Pallas kernels  153 us (97%)
  local copies, waits for them, and re-layouts  3.06 us (2%)
    pallas_call x1, Pallas kernels, fused(): pl.pallas_call(functools.partial(mixer, layers), out_shape=jax.ShapeDtype...  153 us

profile of v3, /device:TPU:0, one launch (start us, length us, event | category | flops | bytes accessed | tf_op | source)
XLA Modules:
  0.0 155.7 jit_solution(14531344814889734617)
XLA Ops:
  0.0 1.3 copy.9.taps
  1.3 152.6 %shard_map.82 = bf16[384,512]{1,0:T(8,128)(2,1)} custom-call(bf16[384,512]{1,0:T(8,128)(2,1)} %x_hbm.1, bf16[2,512,512]{2,1,0:T(8,128)(2,1)} %wi.1, bf16[2,512,512]{2,1,0:T(8,128)(2,1)} %wv.1, bf16[2,512,512]{2,1,0:T(8,128)(2,1)} %wg.1, bf16[2,512,512]{2,1,0:T(8,128)(2,1)} %wo.1, bf16[2,3,512]{2,1,0:T(4,128)(2,1)} %copy.9.taps, f32[2,512]{1,0:T(2,128)} %gain.1, ...), custom_call_target="tpu_custom_call" | custom-call | tf_op jit(solution)/shard_map/pallas_call | solution.py:481
  153.9 1.8 %copy.11 = bf16[384,512]{1,0:T(8,128)(2,1)} copy(bf16[384,512]{1,0:T(8,128)(2,1)} %shard_map.82) | data formatting | bytes 786432

commit v4 on v3

--- a/solution.py
+++ b/solution.py
@@ -152,18 +152,21 @@
 
     @pl.when(is_end)
     def _():
+        local(0).wait()
+        end_piece(0, 0).start()
         x_copy.wait()
         tokens_in().start()
         order = [(0, 0)]
         for u in range(1, units):
             order += [(u, 0), (u - 1, 1)]
         order += [(units - 1, 1)]
-        for u in range(units):
+        for u in range(1, units):
             local(u).wait()
         for n, (u, i) in enumerate(order):
             if n >= 3:
                 end_piece(*order[n - 3]).wait_send()
-            end_piece(u, i).start()
+            if n > 0:
+                end_piece(u, i).start()
         for u, i in order[-3:]:
             end_piece(u, i).wait_send()
         tokens_in().wait_send()

time: 158 us -> 159 us (level)
  no operation moved by 1% of the time
where the time goes in v4:
time: 159 us; the launch traced here: 157 us
  Pallas kernels  154 us (97%)
  local copies, waits for them, and re-layouts  3.06 us (2%)
    pallas_call x1, Pallas kernels, fused(): pl.pallas_call(functools.partial(mixer, layers), out_shape=jax.ShapeDtype...  154 us

profile of v4, /device:TPU:0, one launch (start us, length us, event | category | flops | bytes accessed | tf_op | source)
XLA Modules:
  0.0 156.7 jit_solution(10804317358976106686)
XLA Ops:
  0.0 1.3 copy.9.taps
  1.3 153.6 %shard_map.82 = bf16[384,512]{1,0:T(8,128)(2,1)} custom-call(bf16[384,512]{1,0:T(8,128)(2,1)} %x_hbm.1, bf16[2,512,512]{2,1,0:T(8,128)(2,1)} %wi.1, bf16[2,512,512]{2,1,0:T(8,128)(2,1)} %wv.1, bf16[2,512,512]{2,1,0:T(8,128)(2,1)} %wg.1, bf16[2,512,512]{2,1,0:T(8,128)(2,1)} %wo.1, bf16[2,3,512]{2,1,0:T(4,128)(2,1)} %copy.9.taps, f32[2,512]{1,0:T(2,128)} %gain.1, ...), custom_call_target="tpu_custom_call" | custom-call | tf_op jit(solution)/shard_map/pallas_call | solution.py:484
  154.9 1.8 %copy.11 = bf16[384,512]{1,0:T(8,128)(2,1)} copy(bf16[384,512]{1,0:T(8,128)(2,1)} %shard_map.82) | data formatting | bytes 786432
